TPU v7x, 32 devices: a whole 2x2x4 slice. The times are simulated.
32 devices in a mesh: ep: 16 (over z, y, x), tp: 2 (over core).
Axes of the slice: x: 2, y: 2, z: 4, core: 2. Of those that a mesh axis runs over, the one named last changes fastest.
Arguments:
- tokens: bfloat16 [4096, 1024], P('ep'), may hold values from -6 to 6
- norm_gain: float32 [1024], replicated, may hold values from 0.1 to 1.9
- routing: int32 [4096, 2], P('ep'), may hold values from 0 to 31, all different within a row; in each aligned block of 256 rows (0 to 255, 256 to 511, ...) at most 16 rows name the same one
- route_weights: float32 [4096, 2], P('ep'), may hold values from 0.1 to 1
- lengths: int32 [1024], P('ep'), may hold values from 1 to 4, 2560 in all
- w_gate: bfloat16 [32, 1024, 3584], P('ep', None, 'tp'), may hold values from -0.1875 to 0.1875
- w_up: bfloat16 [32, 1024, 3584], P('ep', None, 'tp'), may hold values from -0.1875 to 0.1875
- w_down: bfloat16 [32, 3584, 1024], P('ep', 'tp'), may hold values from -0.09375 to 0.09375
Outputs:
- mixed: bfloat16 [4096, 1024], P('ep', 'tp')
Inputs may be any that keep to these rules, and one draw needn't show every extreme that they name: `routing`: each row names 2 different experts; at most 16 rows of one device name the same expert, and that many is reached.
All inputs are finite; a program needn't handle non-finite values. No bound on the sum of `lengths` on one device may be relied on, other than what follows from the above.
Results may differ from a plain program's by a relative error of at most 0.009.
Values may be sent and summed in bfloat16 or wider, within the bound.
A program may use at most 64 MiB of HBM per device.

v0:
```python
import functools

import jax
import jax.numpy as jnp
from jax import lax
from jax.experimental import pallas as pl
from jax.experimental.pallas import tpu as pltpu
from jax.sharding import PartitionSpec as P

MESH = pl.DeviceIdType.MESH
GROUPS = 2
TILE = 16
eps = 1e-06
BF = jnp.bfloat16
F32 = jnp.float32


def dot(a, b):
    return jnp.dot(a, b, preferred_element_type=F32)


def kernel(
    n, groups, local, bound, span,
    gain_hbm, routing_hbm, weights_hbm, lengths_hbm,
    tokens_hbm, gate_hbm, up_hbm, down_hbm,
    out_ref,
    gain_ref, routing_ref, weights_ref, lengths_ref, tok, gate_w, up_w, down_w, outgoing, incoming, hidden, partial, theirs, returning, returned, comb,
    small_sem, tok_sem, w_sem, disp_send, disp_recv, fwd_send, fwd_recv, part_send, part_recv, ret_send, ret_recv,
):
    me = lax.axis_index("ep")
    core = lax.axis_index("tp")
    other = 1 - core
    pow2 = n & (n - 1) == 0
    per = n // groups
    rows = per * bound
    group_slots = local * rows
    tok_rows, width = tok.shape
    half = width // 2
    chosen = routing_ref.shape[0]
    experts = n * local
    mine = pl.ds(pl.multiple_of(core * half, half), half)

    def target(k):
        return lax.bitwise_xor(me, k) if pow2 else lax.rem(me + k, n)

    small = [
        pltpu.make_async_copy(src, dst, small_sem.at[i])
        for i, (src, dst) in enumerate((
            (lengths_hbm, lengths_ref),
            (routing_hbm, routing_ref),
            (gain_hbm, gain_ref),
            (weights_hbm, weights_ref),
        ))
    ]
    tok_copy = pltpu.make_async_copy(tokens_hbm, tok, tok_sem)
    tok_copy.start()
    for copy in small:
        copy.start()

    barrier = pltpu.get_barrier_semaphore()
    for k in range(1, n):
        pl.semaphore_signal(barrier, inc=1, device_id=(target(k), core), device_id_type=MESH)
    pl.semaphore_signal(barrier, inc=1, device_id=(me, other), device_id_type=MESH)

    loads = {}
    for x in range(local):
        for i, (src, dst) in enumerate(((gate_hbm, gate_w), (up_hbm, up_w), (down_hbm, down_w))):
            loads[x, i] = pltpu.make_async_copy(src.at[x], dst.at[x], w_sem.at[x, i])
            loads[x, i].start()

    for copy in small:
        copy.wait()

    count = lengths_ref.shape[1]
    spread = (
        lax.broadcasted_iota(jnp.int32, (count, tok_rows), 1) // span
        == lax.broadcasted_iota(jnp.int32, (count, tok_rows), 0)
    ).astype(BF)
    lens = jnp.broadcast_to(lengths_ref[...].astype(F32), (8, count)).astype(BF)
    live_len = dot(lens, spread)[0:1]
    place = lax.broadcasted_iota(jnp.int32, (1, tok_rows), 1) % span
    live = place.astype(F32) < live_len
    routing = routing_ref[...]
    ids = lax.broadcasted_iota(jnp.int32, (experts, tok_rows), 0)
    named = ids == routing[0:1]
    for i in range(1, chosen):
        named = named | (ids == routing[i : i + 1])
    named = named & live
    earlier = (
        lax.broadcasted_iota(jnp.int32, (tok_rows, tok_rows), 0)
        < lax.broadcasted_iota(jnp.int32, (tok_rows, tok_rows), 1)
    ).astype(BF)
    rank = dot(jnp.where(named, 1.0, 0.0).astype(BF), earlier)
    rank = jnp.where(named, rank, -1.0).astype(BF)

    def slot_ids(shape, g):
        s = lax.broadcasted_iota(jnp.int32, shape, 0)
        k = (s // bound) % per * groups + g
        peer = lax.bitwise_xor(jnp.full(shape, me, jnp.int32), k) if pow2 else (me + k) % n
        return peer * local + s // rows, s % bound

    tok_copy.wait()
    floats = tok[...].astype(F32)
    scale = lax.rsqrt(jnp.mean(floats * floats, axis=-1, keepdims=True) + eps)
    normed = (tok[:, mine].astype(F32) * scale * gain_ref[:, mine]).astype(BF)

    def dispatch(k):
        g, j = k % groups, k // groups
        return pltpu.make_async_remote_copy(
            src_ref=outgoing.at[g, :, j],
            dst_ref=incoming.at[g, :, j, :, mine],
            send_sem=disp_send.at[k],
            recv_sem=disp_recv.at[k],
            device_id=(target(k), core),
            device_id_type=MESH,
        )

    def forward(k):
        g, j = k % groups, k // groups
        return pltpu.make_async_remote_copy(
            src_ref=incoming.at[g, :, j, :, mine],
            dst_ref=incoming.at[g, :, j, :, mine],
            send_sem=fwd_send.at[k],
            recv_sem=fwd_recv.at[k],
            device_id=(me, other),
            device_id_type=MESH,
        )

    def swap(g, x):
        return pltpu.make_async_remote_copy(
            src_ref=partial.at[g, x, other],
            dst_ref=theirs.at[g, x],
            send_sem=part_send.at[g, x],
            recv_sem=part_recv.at[g, x],
            device_id=(me, other),
            device_id_type=MESH,
        )

    def give_back(k, x):
        g, j = k % groups, k // groups
        return pltpu.make_async_remote_copy(
            src_ref=returning.at[g, x, j],
            dst_ref=returned.at[g, x, j],
            send_sem=ret_send.at[k, x],
            recv_sem=ret_recv.at[k, x],
            device_id=(target((n - k) % n if not pow2 else k), core),
            device_id_type=MESH,
        )

    def members(g):
        return list(range(g, n, groups))

    def fill(g):
        owner, slot = slot_ids((group_slots, experts), g)
        to_expert = (owner == lax.broadcasted_iota(jnp.int32, (group_slots, experts), 1)).astype(BF)
        owner, slot = slot_ids((group_slots, tok_rows), g)
        hit = dot(to_expert, rank) == slot.astype(F32)
        block = dot(jnp.where(hit, 1.0, 0.0).astype(BF), normed).astype(BF)
        block = block.reshape(local, per, bound, half)
        outgoing[g] = block
        if g == 0:
            incoming[0, :, 0, :, mine] = block[:, 0]

    def send(g):
        for k in reversed(members(g)):
            if k:
                dispatch(k).start()

    fill(0)
    pl.semaphore_wait(barrier, n)
    send(0)
    forward(0).start()
    for g in range(1, groups):
        fill(g)
        send(g)
    for g in range(groups):
        owner, slot = slot_ids((group_slots, experts), g)
        to_expert = (owner == lax.broadcasted_iota(jnp.int32, (group_slots, experts), 1)).astype(BF)
        owner, slot = slot_ids((group_slots, tok_rows), g)
        hit = dot(to_expert, rank) == slot.astype(F32)
        value = jnp.zeros((group_slots, tok_rows), F32)
        for i in range(chosen):
            value = jnp.where(owner == routing[i : i + 1], weights_ref[i : i + 1], value)
        comb[g] = jnp.where(hit, value, 0.0).T

    def arrive(g):
        for k in members(g):
            if k:
                dispatch(k).wait_recv()
                forward(k).start()

    def finish(g, x):
        swap(g, x).wait_recv()
        total = (partial[g, x, core].astype(F32) + theirs[g, x].astype(F32)).astype(BF)
        total = total.reshape(per, bound, half)
        returning[g, x] = total
        if g == 0:
            returned[0, x, 0] = total[0]
        for k in reversed(members(g)):
            if k:
                give_back(k, x).start()

    arrive(0)
    for g in range(groups):
        for k in members(g):
            forward(k).wait_recv()
        for x in range(local):
            xs = incoming[g, x].reshape(rows, width)
            if g == 0:
                loads[x, 0].wait()
            gate = dot(xs, gate_w[x])
            if g == 0:
                loads[x, 1].wait()
            hidden[...] = (gate / (1.0 + jnp.exp(-gate)) * dot(xs, up_w[x])).astype(BF)
            if g == 0:
                loads[x, 2].wait()
            if x:
                finish(g, x - 1)
            down = dot(hidden[...], down_w[x]).astype(BF)
            partial[g, x, 0] = down[:, :half]
            partial[g, x, 1] = down[:, half:]
            swap(g, x).start()
        if g + 1 < groups:
            arrive(g + 1)
        finish(g, local - 1)
    mixed = jnp.zeros((tok_rows, half), F32)
    for g in range(groups):
        for x in range(local):
            for k in members(g):
                if k:
                    give_back(k, x).wait_recv()
        values = returned[g].reshape(group_slots, half)
        weight = comb[g]
        high = weight.astype(BF)
        low = (weight - high.astype(F32)).astype(BF)
        mixed = mixed + dot(high, values) + dot(low, values)
    out_ref[...] = mixed.astype(BF)
    for k in range(n):
        if k:
            dispatch(k).wait_send()
            for x in range(local):
                give_back(k, x).wait_send()
        forward(k).wait_send()
    for g in range(groups):
        for x in range(local):
            swap(g, x).wait_send()


def per_device(n, tokens, norm_gain, routing, route_weights, lengths, w_gate, w_up, w_down):
    local, width, units = w_gate.shape
    tok_rows, chosen = routing.shape
    experts = n * local
    groups = GROUPS
    bound = 2 * ((tok_rows * chosen + 2 * experts - 1) // (2 * experts))
    bound = (bound + TILE - 1) // TILE * TILE
    half = width // 2
    per = n // groups
    rows = per * bound
    span = tok_rows // lengths.shape[0]
    vmem = pl.BlockSpec(memory_space=pltpu.VMEM)
    hbm = pl.BlockSpec(memory_space=pltpu.HBM)
    dma = pltpu.SemaphoreType.DMA
    return pl.pallas_call(
        functools.partial(kernel, n, groups, local, bound, span),
        out_shape=pltpu.VMEM((tok_rows, half), BF),
        in_specs=[hbm] * 8,
        out_specs=vmem,
        scratch_shapes=[
            pltpu.VMEM((1, width), F32),
            pltpu.VMEM((chosen, tok_rows), jnp.int32),
            pltpu.VMEM((chosen, tok_rows), F32),
            pltpu.VMEM((1, lengths.shape[0]), jnp.int32),
            pltpu.VMEM((tok_rows, width), BF),
            pltpu.VMEM((local, width, units), BF),
            pltpu.VMEM((local, width, units), BF),
            pltpu.VMEM((local, units, width), BF),
            pltpu.VMEM((groups, local, per, bound, half), BF),
            pltpu.VMEM((groups, local, per, bound, width), BF),
            pltpu.VMEM((rows, units), BF),
            pltpu.VMEM((groups, local, 2, rows, half), BF),
            pltpu.VMEM((groups, local, rows, half), BF),
            pltpu.VMEM((groups, local, per, bound, half), BF),
            pltpu.VMEM((groups, local, per, bound, half), BF),
            pltpu.VMEM((groups, tok_rows, local * rows), F32),
            dma((4,)),
            dma,
            dma((local, 3)),
            dma((n,)),
            dma((n,)),
            dma((n,)),
            dma((n,)),
            dma((groups, local)),
            dma((groups, local)),
            dma((n, local)),
            dma((n, local)),
        ],
        compiler_params=pltpu.CompilerParams(
            collective_id=0, has_side_effects=True, vmem_limit_bytes=66000000
        ),
    )(
        norm_gain.reshape(1, width),
        routing.T,
        route_weights.T,
        lengths.reshape(1, -1),
        tokens,
        w_gate,
        w_up,
        w_down,
    )


def solution(mesh):
    placed = (
        P("ep", None),
        P(),
        P("ep", None),
        P("ep", None),
        P("ep"),
        P("ep", None, "tp"),
        P("ep", None, "tp"),
        P("ep", "tp", None),
    )
    return jax.shard_map(
        functools.partial(per_device, mesh.shape["ep"]),
        mesh=mesh, in_specs=placed, out_specs=P("ep", "tp"), check_vma=False,
    )
```

profile of v0, /device:TPU:0, one launch (start us, length us, event | category | flops | bytes accessed | tf_op | source)
XLA Modules:
  0.0 36.5 jit_solution(1054721138045430106)
XLA Ops:
  0.0 35.8 %shard_map.82 = bf16[256,512]{1,0:T(8,128)(2,1)S(1)} custom-call(f32[1,1024]{1,0:T(1,128)} %bitcast.4, s32[2,256]{1,0:T(2,128)} %bitcast.5, f32[2,256]{1,0:T(2,128)} %bitcast.6, s32[1,64]{1,0:T(1,128)} %bitcast.7, bf16[256,1024]{1,0:T(8,128)(2,1)} %tokens_hbm.1, bf16[2,1024,1792]{2,1,0:T(8,128)(2,1)} %gate_hbm.1, bf16[2,1024,1792]{2,1,0:T(8,128)(2,1)} %up_hbm.1, ...), custom_call_target="tpu_custom_call" | custom-call | tf_op jit(solution)/shard_map/pallas_call | solution.py:263
  35.8 0.7 %copy.10 = bf16[256,512]{1,0:T(8,128)(2,1)} copy(bf16[256,512]{1,0:T(8,128)(2,1)S(1)} %shard_map.82) | data formatting | bytes 524288
where the time goes:
time: 36.6 us; the launch traced here: 36.5 us
  Pallas kernels  35.8 us (98%)
  local copies, waits for them, and re-layouts  0.71 us (2%)
    pallas_call x1, Pallas kernels, per_device(): pl.pallas_call(functools.partial(kernel, n, groups, local, bound, span),...  35.8 us

commit v1 on v0

v1 whole, which is shorter than its diff:
```python
import functools

import jax
import jax.numpy as jnp
from jax import lax
from jax.experimental import pallas as pl
from jax.experimental.pallas import tpu as pltpu
from jax.sharding import PartitionSpec as P

MESH = pl.DeviceIdType.MESH
PARTS = 4
ORDER = (0, 3, 1, 2)
TILE = 16
eps = 1e-06
BF = jnp.bfloat16
F32 = jnp.float32


def dot(a, b):
    return jnp.dot(a, b, preferred_element_type=F32)


def kernel(
    n, local, bound, span,
    gain_hbm, routing_hbm, weights_hbm, lengths_hbm,
    tokens_hbm, gate_hbm, up_hbm, down_hbm,
    out_ref,
    gain_ref, routing_ref, weights_ref, lengths_ref, tok, gate_w, up_w, down_w, outgoing, incoming, hidden, partial, theirs, returning, returned, comb,
    small_sem, tok_sem, w_sem, ready, disp_send, disp_recv, fwd_send, fwd_recv, part_send, part_recv, ret_send, ret_recv,
):
    me = lax.axis_index("ep")
    core = lax.axis_index("tp")
    other = 1 - core
    per = n // PARTS
    rows = per * bound
    slots = local * rows
    tok_rows, width = tok.shape
    half = width // 2
    chosen = routing_ref.shape[0]
    experts = n * local
    mine = pl.ds(pl.multiple_of(core * half, half), half)
    quarter = me // per
    inner = jnp.logical_or(quarter == 1, quarter == 2)

    def target(k):
        return lax.bitwise_xor(me, k)

    def members(q):
        return [k for k in range(q * per, (q + 1) * per) if k]

    small = [
        pltpu.make_async_copy(src, dst, small_sem.at[i])
        for i, (src, dst) in enumerate((
            (lengths_hbm, lengths_ref),
            (routing_hbm, routing_ref),
            (gain_hbm, gain_ref),
            (weights_hbm, weights_ref),
        ))
    ]
    tok_copy = pltpu.make_async_copy(tokens_hbm, tok, tok_sem)
    tok_copy.start()
    for copy in small:
        copy.start()

    barrier = pltpu.get_barrier_semaphore()

    def greet(sem, q):
        for k in members(q):
            pl.semaphore_signal(sem, inc=1, device_id=(target(k), core), device_id_type=MESH)

    pl.semaphore_signal(barrier, inc=1, device_id=(me, other), device_id_type=MESH)
    greet(barrier, 3)

    @pl.when(inner)
    def _():
        greet(barrier, 2)
        greet(barrier, 1)

    greet(barrier, 0)

    loads = {}
    for x in range(local):
        for i, (src, dst) in enumerate(((gate_hbm, gate_w), (up_hbm, up_w), (down_hbm, down_w))):
            loads[x, i] = pltpu.make_async_copy(src.at[x], dst.at[x], w_sem.at[x, i])
            loads[x, i].start()

    for copy in small:
        copy.wait()

    count = lengths_ref.shape[1]
    spread = (
        lax.broadcasted_iota(jnp.int32, (count, tok_rows), 1) // span
        == lax.broadcasted_iota(jnp.int32, (count, tok_rows), 0)
    ).astype(BF)
    lens = jnp.broadcast_to(lengths_ref[...].astype(F32), (8, count)).astype(BF)
    live_len = dot(lens, spread)[0:1]
    place = lax.broadcasted_iota(jnp.int32, (1, tok_rows), 1) % span
    live = place.astype(F32) < live_len
    routing = routing_ref[...]
    ids = lax.broadcasted_iota(jnp.int32, (experts, tok_rows), 0)
    named = ids == routing[0:1]
    for i in range(1, chosen):
        named = named | (ids == routing[i : i + 1])
    named = named & live
    earlier = (
        lax.broadcasted_iota(jnp.int32, (tok_rows, tok_rows), 0)
        < lax.broadcasted_iota(jnp.int32, (tok_rows, tok_rows), 1)
    ).astype(BF)
    rank = dot(jnp.where(named, 1.0, 0.0).astype(BF), earlier)
    rank = jnp.where(named, rank, -1.0).astype(BF)

    def slot_ids(shape, q):
        s = lax.broadcasted_iota(jnp.int32, shape, 0)
        k = (s // bound) % per + q * per
        peer = lax.bitwise_xor(jnp.full(shape, me, jnp.int32), k)
        return peer * local + s // rows, s % bound

    def find(q):
        owner, slot = slot_ids((slots, experts), q)
        to_expert = (owner == lax.broadcasted_iota(jnp.int32, (slots, experts), 1)).astype(BF)
        owner, slot = slot_ids((slots, tok_rows), q)
        return owner, dot(to_expert, rank) == slot.astype(F32)

    tok_copy.wait()
    floats = tok[...].astype(F32)
    scale = lax.rsqrt(jnp.mean(floats * floats, axis=-1, keepdims=True) + eps)
    normed = (tok[:, mine].astype(F32) * scale * gain_ref[:, mine]).astype(BF)

    def remote(src, dst, send, recv, device):
        return pltpu.make_async_remote_copy(
            src_ref=src, dst_ref=dst, send_sem=send, recv_sem=recv,
            device_id=device, device_id_type=MESH,
        )

    partner = (me, other)

    def landed(ref, q):
        return ref.at[q, :, 1:] if q == 0 else ref.at[q]

    def dispatch(k):
        q, j = k // per, k % per
        return remote(
            outgoing.at[q, :, j], incoming.at[q, :, j, :, mine],
            disp_send.at[q], disp_recv.at[q], (target(k), core),
        )

    def forward(q):
        view = incoming.at[q, :, :, :, mine]
        return remote(view, view, fwd_send.at[q], fwd_recv.at[q], partner)

    def swap(q, x):
        return remote(
            partial.at[q, x, other], theirs.at[q, x],
            part_send.at[q, x], part_recv.at[q, x], partner,
        )

    def give_back(k, x):
        q, j = k // per, k % per
        return remote(
            returning.at[q, x, j], returned.at[q, x, j],
            ret_send.at[q], ret_recv.at[q], (target(k), core),
        )

    def fill(q):
        hit = find(q)[1]
        block = dot(jnp.where(hit, 1.0, 0.0).astype(BF), normed).astype(BF)
        block = block.reshape(local, per, bound, half)
        outgoing[q] = block
        if q == 0:
            incoming[0, :, 0, :, mine] = block[:, 0]

    def send(q):
        for k in reversed(members(q)):
            dispatch(k).start()

    fill(3)
    pl.semaphore_wait(barrier, jnp.where(inner, 2 * per, 4 * per))

    @pl.when(jnp.logical_not(inner))
    def _():
        greet(ready, 1)
        greet(ready, 2)

    send(3)
    fill(0)
    send(0)
    fill(1)
    fill(2)
    for q in range(PARTS):
        owner, hit = find(q)
        value = jnp.zeros((slots, tok_rows), F32)
        for i in range(chosen):
            value = jnp.where(owner == routing[i : i + 1], weights_ref[i : i + 1], value)
        comb[q] = jnp.where(hit, value, 0.0).T

    @pl.when(inner)
    def _():
        pl.semaphore_wait(ready, 2 * per)

    send(1)
    send(2)

    def arrive(q):
        view = landed(incoming, q).at[..., mine]
        remote(view, view, disp_send.at[q], disp_recv.at[q], partner).wait_recv()
        forward(q).start()

    def finish(q, x):
        swap(q, x).wait_recv()
        total = (partial[q, x, core].astype(F32) + theirs[q, x].astype(F32)).astype(BF)
        total = total.reshape(per, bound, half)
        returning[q, x] = total
        if q == 0:
            returned[0, x, 0] = total[0]
        for k in reversed(members(q)):
            give_back(k, x).start()

    arrive(ORDER[0])
    pending = None
    first = True
    for i, q in enumerate(ORDER):
        forward(q).wait_recv()
        for x in range(local):
            xs = incoming[q, x].reshape(rows, width)
            if first:
                loads[x, 0].wait()
            gate = dot(xs, gate_w[x])
            if first:
                loads[x, 1].wait()
            hidden[...] = (gate / (1.0 + jnp.exp(-gate)) * dot(xs, up_w[x])).astype(BF)
            if first:
                loads[x, 2].wait()
            if pending:
                finish(*pending)
            down = dot(hidden[...], down_w[x]).astype(BF)
            partial[q, x, 0] = down[:, :half]
            partial[q, x, 1] = down[:, half:]
            swap(q, x).start()
            pending = (q, x)
        first = False
        if i + 1 < PARTS:
            arrive(ORDER[i + 1])
    finish(*pending)

    mixed = jnp.zeros((tok_rows, half), F32)
    for q in (0, 1, 3, 2):
        view = landed(returned, q)
        remote(view, view, ret_send.at[q], ret_recv.at[q], partner).wait_recv()
        values = returned[q].reshape(slots, half)
        weight = comb[q]
        high = weight.astype(BF)
        low = (weight - high.astype(F32)).astype(BF)
        mixed = mixed + dot(high, values) + dot(low, values)
    out_ref[...] = mixed.astype(BF)
    for q in range(PARTS):
        view = landed(outgoing, q)
        remote(view, view, disp_send.at[q], disp_recv.at[q], partner).wait_send()
        view = landed(returning, q)
        remote(view, view, ret_send.at[q], ret_recv.at[q], partner).wait_send()
        forward(q).wait_send()
        for x in range(local):
            swap(q, x).wait_send()


def per_device(n, tokens, norm_gain, routing, route_weights, lengths, w_gate, w_up, w_down):
    local, width, units = w_gate.shape
    tok_rows, chosen = routing.shape
    experts = n * local
    bound = 2 * ((tok_rows * chosen + 2 * experts - 1) // (2 * experts))
    bound = (bound + TILE - 1) // TILE * TILE
    half = width // 2
    per = n // PARTS
    rows = per * bound
    span = tok_rows // lengths.shape[0]
    vmem = pl.BlockSpec(memory_space=pltpu.VMEM)
    hbm = pl.BlockSpec(memory_space=pltpu.HBM)
    dma = pltpu.SemaphoreType.DMA
    return pl.pallas_call(
        functools.partial(kernel, n, local, bound, span),
        out_shape=pltpu.VMEM((tok_rows, half), BF),
        in_specs=[hbm] * 8,
        out_specs=vmem,
        scratch_shapes=[
            pltpu.VMEM((1, width), F32),
            pltpu.VMEM((chosen, tok_rows), jnp.int32),
            pltpu.VMEM((chosen, tok_rows), F32),
            pltpu.VMEM((1, lengths.shape[0]), jnp.int32),
            pltpu.VMEM((tok_rows, width), BF),
            pltpu.VMEM((local, width, units), BF),
            pltpu.VMEM((local, width, units), BF),
            pltpu.VMEM((local, units, width), BF),
            pltpu.VMEM((PARTS, local, per, bound, half), BF),
            pltpu.VMEM((PARTS, local, per, bound, width), BF),
            pltpu.VMEM((rows, units), BF),
            pltpu.VMEM((PARTS, local, 2, rows, half), BF),
            pltpu.VMEM((PARTS, local, rows, half), BF),
            pltpu.VMEM((PARTS, local, per, bound, half), BF),
            pltpu.VMEM((PARTS, local, per, bound, half), BF),
            pltpu.VMEM((PARTS, tok_rows, local * rows), F32),
            dma((4,)),
            dma,
            dma((local, 3)),
            pltpu.SemaphoreType.REGULAR,
            dma((PARTS,)),
            dma((PARTS,)),
            dma((PARTS,)),
            dma((PARTS,)),
            dma((PARTS, local)),
            dma((PARTS, local)),
            dma((PARTS,)),
            dma((PARTS,)),
        ],
        compiler_params=pltpu.CompilerParams(
            collective_id=0, has_side_effects=True, vmem_limit_bytes=66000000
        ),
    )(
        norm_gain.reshape(1, width),
        routing.T,
        route_weights.T,
        lengths.reshape(1, -1),
        tokens,
        w_gate,
        w_up,
        w_down,
    )


def solution(mesh):
    placed = (
        P("ep", None),
        P(),
        P("ep", None),
        P("ep", None),
        P("ep"),
        P("ep", None, "tp"),
        P("ep", None, "tp"),
        P("ep", "tp", None),
    )
    return jax.shard_map(
        functools.partial(per_device, mesh.shape["ep"]),
        mesh=mesh, in_specs=placed, out_specs=P("ep", "tp"), check_vma=False,
    )
```

time: 36.6 us -> 40.8 us (1.11)
  Pallas kernels: 35.8 us -> 39.9 us
    pallas_call x1, Pallas kernels: 35.8 us -> 39.9 us  [per_device(): pl.pallas_call(functools.partial(kernel, n, local, bound, span), out_shap...]
where the time goes in v1:
time: 40.8 us; the launch traced here: 40.7 us
  Pallas kernels  39.9 us (98%)
  local copies, waits for them, and re-layouts  0.71 us (2%)
    pallas_call x1, Pallas kernels, per_device(): pl.pallas_call(functools.partial(kernel, n, local, bound, span), out_shap...  39.9 us

profile of v1, /device:TPU:0, one launch (start us, length us, event | category | flops | bytes accessed | tf_op | source)
XLA Modules:
  0.0 40.7 jit_solution(10906750746572546224)
XLA Ops:
  0.0 39.9 %shard_map.82 = bf16[256,512]{1,0:T(8,128)(2,1)S(1)} custom-call(f32[1,1024]{1,0:T(1,128)} %bitcast.4, s32[2,256]{1,0:T(2,128)} %bitcast.5, f32[2,256]{1,0:T(2,128)} %bitcast.6, s32[1,64]{1,0:T(1,128)} %bitcast.7, bf16[256,1024]{1,0:T(8,128)(2,1)} %tokens_hbm.1, bf16[2,1024,1792]{2,1,0:T(8,128)(2,1)} %gate_hbm.1, bf16[2,1024,1792]{2,1,0:T(8,128)(2,1)} %up_hbm.1, ...), custom_call_target="tpu_custom_call" | custom-call | tf_op jit(solution)/shard_map/pallas_call | solution.py:278
  40.0 0.7 %copy.10 = bf16[256,512]{1,0:T(8,128)(2,1)} copy(bf16[256,512]{1,0:T(8,128)(2,1)S(1)} %shard_map.82) | data formatting | bytes 524288

commit v2 on v1

--- a/solution.py
+++ b/solution.py
@@ -9,7 +9,8 @@
 
 MESH = pl.DeviceIdType.MESH
 PARTS = 4
-ORDER = (0, 3, 1, 2)
+GROUPS = ((0, 3), (1, 2))
+PLACE = {q: (g, i) for g, qs in enumerate(GROUPS) for i, q in enumerate(qs)}
 TILE = 16
 eps = 1e-06
 BF = jnp.bfloat16
@@ -34,6 +35,7 @@
     per = n // PARTS
     rows = per * bound
     slots = local * rows
+    most = hidden.shape[0]
     tok_rows, width = tok.shape
     half = width // 2
     chosen = routing_ref.shape[0]
@@ -86,6 +88,7 @@
 
     for copy in small:
         copy.wait()
+    tok_copy.wait()
 
     count = lengths_ref.shape[1]
     spread = (
@@ -121,7 +124,6 @@
         owner, slot = slot_ids((slots, tok_rows), q)
         return owner, dot(to_expert, rank) == slot.astype(F32)
 
-    tok_copy.wait()
     floats = tok[...].astype(F32)
     scale = lax.rsqrt(jnp.mean(floats * floats, axis=-1, keepdims=True) + eps)
     normed = (tok[:, mine].astype(F32) * scale * gain_ref[:, mine]).astype(BF)
@@ -135,29 +137,35 @@
     partner = (me, other)
 
     def landed(ref, q):
-        return ref.at[q, :, 1:] if q == 0 else ref.at[q]
+        g, i = PLACE[q]
+        return ref.at[g, :, i, 1:] if q == 0 else ref.at[g, :, i]
+
+    def at(q, j):
+        g, i = PLACE[q]
+        return g, slice(None), i, j
 
     def dispatch(k):
         q, j = k // per, k % per
         return remote(
-            outgoing.at[q, :, j], incoming.at[q, :, j, :, mine],
+            outgoing.at[*at(q, j)], incoming.at[*at(q, j), :, mine],
             disp_send.at[q], disp_recv.at[q], (target(k), core),
         )
 
     def forward(q):
-        view = incoming.at[q, :, :, :, mine]
+        view = incoming.at[*at(q, slice(None)), :, mine]
         return remote(view, view, fwd_send.at[q], fwd_recv.at[q], partner)
 
-    def swap(q, x):
+    def swap(g, x):
         return remote(
-            partial.at[q, x, other], theirs.at[q, x],
-            part_send.at[q, x], part_recv.at[q, x], partner,
+            partial.at[g, x, other], theirs.at[g, x],
+            part_send.at[g, x], part_recv.at[g, x], partner,
         )
 
     def give_back(k, x):
         q, j = k // per, k % per
+        g, i = PLACE[q]
         return remote(
-            returning.at[q, x, j], returned.at[q, x, j],
+            returning.at[g, x, i, j], returned.at[g, x, i, j],
             ret_send.at[q], ret_recv.at[q], (target(k), core),
         )
 
@@ -165,9 +173,9 @@
         hit = find(q)[1]
         block = dot(jnp.where(hit, 1.0, 0.0).astype(BF), normed).astype(BF)
         block = block.reshape(local, per, bound, half)
-        outgoing[q] = block
+        outgoing[at(q, slice(None))] = block
         if q == 0:
-            incoming[0, :, 0, :, mine] = block[:, 0]
+            incoming[*at(0, 0), :, mine] = block[:, 0]
 
     def send(q):
         for k in reversed(members(q)):
@@ -176,81 +184,108 @@
     fill(3)
     pl.semaphore_wait(barrier, jnp.where(inner, 2 * per, 4 * per))
 
+    @pl.when(inner)
+    def _():
+        send(3)
+
     @pl.when(jnp.logical_not(inner))
     def _():
         greet(ready, 1)
         greet(ready, 2)
 
-    send(3)
     fill(0)
     send(0)
     fill(1)
+
+    @pl.when(jnp.logical_not(inner))
+    def _():
+        send(3)
+        send(1)
+
     fill(2)
+
+    @pl.when(jnp.logical_not(inner))
+    def _():
+        send(2)
+
     for q in range(PARTS):
         owner, hit = find(q)
         value = jnp.zeros((slots, tok_rows), F32)
         for i in range(chosen):
             value = jnp.where(owner == routing[i : i + 1], weights_ref[i : i + 1], value)
-        comb[q] = jnp.where(hit, value, 0.0).T
+        value = jnp.where(hit, value, 0.0).T
+        high = value.astype(BF)
+        comb[q, :, :slots] = high
+        comb[q, :, slots:] = (value - high.astype(F32)).astype(BF)
 
     @pl.when(inner)
     def _():
         pl.semaphore_wait(ready, 2 * per)
-
-    send(1)
-    send(2)
+        send(1)
+        send(2)
 
     def arrive(q):
         view = landed(incoming, q).at[..., mine]
         remote(view, view, disp_send.at[q], disp_recv.at[q], partner).wait_recv()
         forward(q).start()
 
-    def finish(q, x):
-        swap(q, x).wait_recv()
-        total = (partial[q, x, core].astype(F32) + theirs[q, x].astype(F32)).astype(BF)
-        total = total.reshape(per, bound, half)
-        returning[q, x] = total
-        if q == 0:
-            returned[0, x, 0] = total[0]
-        for k in reversed(members(q)):
-            give_back(k, x).start()
-
-    arrive(ORDER[0])
+    def finish(g, x):
+        swap(g, x).wait_recv()
+        total = (partial[g, x, core].astype(F32) + theirs[g, x].astype(F32)).astype(BF)
+        total = total.reshape(len(GROUPS[g]), per, bound, half)
+        returning[g, x] = total
+        if 0 in GROUPS[g]:
+            i = PLACE[0][1]
+            returned[g, x, i, 0] = total[i, 0]
+        def answer(qs):
+            for q in qs:
+                for k in reversed(members(q)):
+                    give_back(k, x).start()
+
+        if g == 0:
+            answer((3, 0))
+            return
+
+        @pl.when(inner)
+        def _():
+            answer((2, 1))
+
+        @pl.when(jnp.logical_not(inner))
+        def _():
+            answer((1, 2))
+
+    for q in GROUPS[0]:
+        arrive(q)
     pending = None
-    first = True
-    for i, q in enumerate(ORDER):
-        forward(q).wait_recv()
+    for g, qs in enumerate(GROUPS):
+        for q in qs:
+            forward(q).wait_recv()
         for x in range(local):
-            xs = incoming[q, x].reshape(rows, width)
-            if first:
-                loads[x, 0].wait()
+            xs = incoming[g, x].reshape(most, width)
+            if g == 0:
+                for i in range(3):
+                    loads[x, i].wait()
             gate = dot(xs, gate_w[x])
-            if first:
-                loads[x, 1].wait()
             hidden[...] = (gate / (1.0 + jnp.exp(-gate)) * dot(xs, up_w[x])).astype(BF)
-            if first:
-                loads[x, 2].wait()
             if pending:
                 finish(*pending)
             down = dot(hidden[...], down_w[x]).astype(BF)
-            partial[q, x, 0] = down[:, :half]
-            partial[q, x, 1] = down[:, half:]
-            swap(q, x).start()
-            pending = (q, x)
-        first = False
-        if i + 1 < PARTS:
-            arrive(ORDER[i + 1])
-    finish(*pending)
+            partial[g, x, 0] = down[:, :half]
+            partial[g, x, 1] = down[:, half:]
+            swap(g, x).start()
+            pending = (g, x)
+        if g + 1 < len(GROUPS):
+            for q in GROUPS[g + 1]:
+                arrive(q)
+        finish(*pending)
+        pending = None
 
     mixed = jnp.zeros((tok_rows, half), F32)
     for q in (0, 1, 3, 2):
         view = landed(returned, q)
         remote(view, view, ret_send.at[q], ret_recv.at[q], partner).wait_recv()
-        values = returned[q].reshape(slots, half)
-        weight = comb[q]
-        high = weight.astype(BF)
-        low = (weight - high.astype(F32)).astype(BF)
-        mixed = mixed + dot(high, values) + dot(low, values)
+        values = returned[at(q, slice(None))].reshape(slots, half)
+        mixed = mixed + dot(comb[q], jnp.concatenate((values, values)))
     out_ref[...] = mixed.astype(BF)
     for q in range(PARTS):
         view = landed(outgoing, q)
@@ -258,8 +293,9 @@
         view = landed(returning, q)
         remote(view, view, ret_send.at[q], ret_recv.at[q], partner).wait_send()
         forward(q).wait_send()
+    for g in range(len(GROUPS)):
         for x in range(local):
-            swap(q, x).wait_send()
+            swap(g, x).wait_send()
 
 
 def per_device(n, tokens, norm_gain, routing, route_weights, lengths, w_gate, w_up, w_down):
@@ -271,6 +307,7 @@
     half = width // 2
     per = n // PARTS
     rows = per * bound
+    groups, deep = len(GROUPS), len(GROUPS[0])
     span = tok_rows // lengths.shape[0]
     vmem = pl.BlockSpec(memory_space=pltpu.VMEM)
     hbm = pl.BlockSpec(memory_space=pltpu.HBM)
@@ -289,14 +326,14 @@
             pltpu.VMEM((local, width, units), BF),
             pltpu.VMEM((local, width, units), BF),
             pltpu.VMEM((local, units, width), BF),
-            pltpu.VMEM((PARTS, local, per, bound, half), BF),
-            pltpu.VMEM((PARTS, local, per, bound, width), BF),
-            pltpu.VMEM((rows, units), BF),
-            pltpu.VMEM((PARTS, local, 2, rows, half), BF),
-            pltpu.VMEM((PARTS, local, rows, half), BF),
-            pltpu.VMEM((PARTS, local, per, bound, half), BF),
-            pltpu.VMEM((PARTS, local, per, bound, half), BF),
-            pltpu.VMEM((PARTS, tok_rows, local * rows), F32),
+            pltpu.VMEM((groups, local, deep, per, bound, half), BF),
+            pltpu.VMEM((groups, local, deep, per, bound, width), BF),
+            pltpu.VMEM((deep * rows, units), BF),
+            pltpu.VMEM((groups, local, 2, deep * rows, half), BF),
+            pltpu.VMEM((groups, local, deep * rows, half), BF),
+            pltpu.VMEM((groups, local, deep, per, bound, half), BF),
+            pltpu.VMEM((groups, local, deep, per, bound, half), BF),
+            pltpu.VMEM((PARTS, tok_rows, 2 * local * rows), BF),
             dma((4,)),
             dma,
             dma((local, 3)),
@@ -305,8 +342,8 @@
             dma((PARTS,)),
             dma((PARTS,)),
             dma((PARTS,)),
-            dma((PARTS, local)),
-            dma((PARTS, local)),
+            dma((groups, local)),
+            dma((groups, local)),
             dma((PARTS,)),
             dma((PARTS,)),
         ],

time: 40.8 us -> 32.3 us (0.79)
  Pallas kernels: 39.9 us -> 31.4 us
    pallas_call x1, Pallas kernels: 39.9 us -> 31.4 us  [per_device(): pl.pallas_call(functools.partial(kernel, n, local, bound, span), out_shap...]
where the time goes in v2:
time: 32.3 us; the launch traced here: 32.1 us
  Pallas kernels  31.4 us (97%)
  local copies, waits for them, and re-layouts  0.71 us (2%)
    pallas_call x1, Pallas kernels, per_device(): pl.pallas_call(functools.partial(kernel, n, local, bound, span), out_shap...  31.4 us
    unnamed x1, local copies, waits for them, and re-layouts  0.71 us

profile of v2, /device:TPU:0, one launch (start us, length us, event | category | flops | bytes accessed | tf_op | source)
XLA Modules:
  0.0 32.1 jit_solution(16410563391585045948)
XLA Ops:
  0.0 31.4 %shard_map.82 = bf16[256,512]{1,0:T(8,128)(2,1)S(1)} custom-call(f32[1,1024]{1,0:T(1,128)} %bitcast.4, s32[2,256]{1,0:T(2,128)} %bitcast.5, f32[2,256]{1,0:T(2,128)} %bitcast.6, s32[1,64]{1,0:T(1,128)} %bitcast.7, bf16[256,1024]{1,0:T(8,128)(2,1)} %tokens_hbm.1, bf16[2,1024,1792]{2,1,0:T(8,128)(2,1)} %gate_hbm.1, bf16[2,1024,1792]{2,1,0:T(8,128)(2,1)} %up_hbm.1, ...), custom_call_target="tpu_custom_call" | custom-call | tf_op jit(solution)/shard_map/pallas_call | solution.py:315
  31.4 0.7 %copy.10 = bf16[256,512]{1,0:T(8,128)(2,1)} copy(bf16[256,512]{1,0:T(8,128)(2,1)S(1)} %shard_map.82) | data formatting | bytes 524288
